TPU v7x, 32 devices: a whole 2x2x4 slice. The times are simulated.
32 devices in a mesh: sp: 16 (over z, y, core), fs: 1, tp: 2 (over x).
Axes of the slice: x: 2, y: 2, z: 4, core: 2. Of those that a mesh axis runs over, the one named last changes fastest.
Arguments:
- tokens: bfloat16 [1, 4096, 2048], P('fs', 'sp'), may hold values from -6 to 6
- norm_gain: float32 [2048], replicated, may hold values from 0.1 to 1.9
- w_state_in: bfloat16 [2048, 1024], P(('sp', 'fs'), 'tp'), may hold values from -0.125 to 0.125
- w_value: bfloat16 [2048, 1024], P(('sp', 'fs'), 'tp'), may hold values from -0.125 to 0.125
- w_outer: bfloat16 [2048, 1024], P(('sp', 'fs'), 'tp'), may hold values from -0.125 to 0.125
- w_inner: bfloat16 [2048, 1024], P(('sp', 'fs'), 'tp'), may hold values from -0.125 to 0.125
- w_state_out: bfloat16 [2048, 1024], P(('sp', 'fs'), 'tp'), may hold values from -0.125 to 0.125
- w_conv_out: bfloat16 [2048, 1024], P(('sp', 'fs'), 'tp'), may hold values from -0.125 to 0.125
- log_step: float32 [64], P('tp'), may hold values from -4.6 to -3.2
- decay_real: float32 [64, 64], P('tp'), may hold values from -5 to 0
- frequency: float32 [64, 64], P('tp'), may hold values from 1 to 192
- step_rate: float32 [1, 4096], P('fs', 'sp'), may hold values from 0.4 to 2.5
- input_real: float32 [64, 64, 16], P('tp'), may hold values from -1 to 1
- input_imag: float32 [64, 64, 16], P('tp'), may hold values from -1 to 1
- read_real: float32 [64, 16, 64], P('tp'), may hold values from -0.75 to 0.75
- read_imag: float32 [64, 16, 64], P('tp'), may hold values from -0.75 to 0.75
- skip_gain: float32 [64, 16], P('tp'), may hold values from -4 to 4
- conv_taps: float32 [3, 1024], P(None, 'tp'), may hold values from -3.5 to 3.5
- initial_state: float32 [1, 2, 64, 64], P('fs', None, 'tp'), may hold values from -6 to 6
Outputs:
- mixed: bfloat16 [1, 4096, 2048], P('fs', ('sp', 'tp'))
- final_state: float32 [1, 2, 64, 64], P('fs', None, 'tp', 'sp')
All inputs are finite; a program needn't handle non-finite values.
Results may differ from a plain program's by a relative error of at most 0.018.
Values may be sent and summed in bfloat16 or wider, within the bound.
A program may use at most 64 MiB of HBM per device.

v0:
```python
import math

import jax
import jax.numpy as jnp
from jax import lax
from jax.experimental import pallas as pl
from jax.experimental.pallas import tpu as pltpu
from jax.sharding import PartitionSpec as P

F32 = jnp.float32
BF16 = jnp.bfloat16
SUB = 8
SIN = (3.1415925798055846, -5.16770686616794, 2.5500311935192803, -0.5980441939118888, 0.07721838615680923)
COS = (0.9999999997799038, -4.93480213707883, 4.058709159556464, -1.335212003052184, 0.2349373138245546, -0.024396324364378108)


def poly(coeffs, z):
    total = coeffs[-1]
    for c in coeffs[-2::-1]:
        total = total * z + c
    return total


def dot(a, b, dims=((1,), (0,))):
    return lax.dot_general(a, b, (dims, ((), ())), preferred_element_type=F32)


def iota(shape, dim):
    return lax.broadcasted_iota(jnp.int32, shape, dim)


def exact(a, b, dims=((1,), (0,))):
    return lax.dot_general(a, b, (dims, ((), ())), precision=lax.Precision.HIGHEST, preferred_element_type=F32)


def cmul(ar, ai, br, bi):
    return ar * br - ai * bi, ar * bi + ai * br


def permutation(rows):
    run = rows // SUB
    r, t = iota((rows, rows), 0), iota((rows, rows), 1)
    return jnp.where((r % SUB) * run + r // SUB == t, 1.0, 0.0).astype(BF16)


def spread(mat, block, width, span, group, states):
    chans = slice(block * width, (block + 1) * width)
    tile = jnp.where(iota((states, span), 0) == iota((states, span), 1) % states, 1.0, 0.0).astype(BF16)
    keep = iota((width, span), 0) // group == iota((width, span), 1) // states
    return jnp.where(keep, dot(mat[chans, :], tile), 0.0).astype(BF16)


def couple(block, state_p, in_r, in_i, dr_ref, di_ref, group, states):
    width = state_p.shape[1]
    span = width // group * states
    cols = slice(block * span, (block + 1) * span)
    for src, dst in ((in_r, dr_ref), (in_i, di_ref)):
        dst[:, cols] = dot(state_p, spread(src, block, width, span, group, states))


def scan_block(lo, span, rate, coef, hr, hi, ar, ai):
    cols = pl.ds(lo, span)
    run = rate.shape[0] // SUB
    reps = span // 128
    decay = jnp.broadcast_to(coef[0:1, cols], (SUB, span))
    turn = jnp.broadcast_to(coef[1:2, cols], (SUB, span))

    def one(j, carry):
        h_r, h_i, a_r, a_i = carry
        at = pl.ds(pl.multiple_of(j * SUB, SUB), SUB)
        r = jnp.concatenate([rate[at, :]] * reps, axis=1)
        u = r * turn
        f = u - jnp.floor(u + 0.5)
        z = f * f
        s = f * poly(SIN, z)
        c = poly(COS, z)
        grow = jnp.exp(r * decay)
        gs = 2.0 * grow * s
        b_r = grow - gs * s
        b_i = gs * c
        p_r, p_i = cmul(b_r - 1.0, b_i, hr[at, cols], hi[at, cols])
        m_r, m_i = cmul(b_r, b_i, h_r, h_i)
        h_r, h_i = m_r + p_r, m_i + p_i
        a_r, a_i = cmul(b_r, b_i, a_r, a_i)
        hr[at, cols] = h_r
        hi[at, cols] = h_i
        ar[at, cols] = a_r
        ai[at, cols] = a_i
        return h_r, h_i, a_r, a_i

    zero = jnp.zeros((SUB, span), F32)
    lax.fori_loop(0, run, one, (zero, zero, zero + 1.0, zero), unroll=2)


def chain_subs(hr, hi, ar, ai, pre, summ):
    rows, flat = hr.shape
    last = rows - SUB
    m_r, m_i = jnp.ones((1, flat), F32), jnp.zeros((1, flat), F32)
    v_r, v_i = jnp.zeros((1, flat), F32), jnp.zeros((1, flat), F32)
    for s in range(SUB):
        row = slice(s, s + 1)
        pre[0, row, :], pre[1, row, :], pre[2, row, :], pre[3, row, :] = m_r, m_i, v_r, v_i
        at = slice(last + s, last + s + 1)
        e_r, e_i = ar[at, :], ai[at, :]
        m_r, m_i = cmul(e_r, e_i, m_r, m_i)
        w_r, w_i = cmul(e_r, e_i, v_r, v_i)
        v_r, v_i = w_r + hr[at, :], w_i + hi[at, :]
    summ[0:1, :], summ[1:2, :], summ[2:3, :], summ[3:4, :] = m_r, m_i, v_r, v_i


def enter(g, s_r, s_i):
    t_r, t_i = cmul(g[0:1, :], g[1:2, :], s_r, s_i)
    return t_r + g[2:3, :], t_i + g[3:4, :]


def join(first, second):
    g_r, g_i = second[0:1, :], second[1:2, :]
    m_r, m_i = cmul(g_r, g_i, first[0:1, :], first[1:2, :])
    w_r, w_i = cmul(g_r, g_i, first[2:3, :], first[3:4, :])
    return jnp.concatenate([m_r, m_i, w_r + second[2:3, :], w_i + second[3:4, :]], axis=0)


def readout(block, width, state_p, enter, hr, hi, ar, ai, pre, rd_r, rd_i, skip, perm, out, group, states):
    span = width // group * states
    cols = slice(block * span, (block + 1) * span)
    chans = slice(block * width, (block + 1) * width)
    rows = hr.shape[0]
    run = rows // SUB
    e_r, e_i = cmul(pre[0, :, cols], pre[1, :, cols], enter[0][:, cols], enter[1][:, cols])
    e_r, e_i = e_r + pre[2, :, cols], e_i + pre[3, :, cols]
    g_r = spread(rd_r, block, width, span, group, states)
    g_i = spread(rd_i, block, width, span, group, states)

    def fixed(local, a, b, sign):
        a3, b3 = a[:, cols].reshape(run, SUB, span), b[:, cols].reshape(run, SUB, span)
        x, y = (e_r, e_i) if sign < 0 else (e_i, e_r)
        shift = a3 * x[None] + (b3 * y[None] if sign > 0 else -b3 * y[None])
        return (local[:, cols].reshape(run, SUB, span) + shift).reshape(rows, span).astype(BF16)

    total = dot(fixed(hr, ar, ai, -1), g_r, ((1,), (1,))) - dot(fixed(hi, ar, ai, 1), g_i, ((1,), (1,)))
    v = total + skip[:, chans] * state_p[:, chans].astype(F32)
    mix = 0.5 * v * (1.0 + jnp.tanh(0.7978845608 * (v + 0.044715 * (v * v * v))))
    out[:, chans] = dot(perm, mix.astype(BF16), ((0,), (0,))).astype(BF16)


def prepare_rates(step_rate, rate):
    rows = rate.shape[0]
    run = rows // SUB
    r, t = iota((rows, rows), 0), iota((rows, rows), 1)
    chosen = jnp.where((r % SUB) * run + r // SUB == t, jnp.broadcast_to(step_rate[...], (rows, rows)), 0.0)
    rate[...] = exact(chosen, jnp.ones((rows, 128), F32))


def flatten(parts, states):
    groups = parts[0].shape[0]
    flat = groups * states
    tile = jnp.where(iota((states, flat), 0) == iota((states, flat), 1) % states, 1.0, 0.0)
    keep = iota((groups, flat), 0) == iota((groups, flat), 1) // states
    return [jnp.sum(jnp.where(keep, exact(part, tile), 0.0), axis=0, keepdims=True) for part in parts]


def prepare_base(log_step, groups):
    base = jnp.where(iota((groups, groups), 0) == iota((groups, groups), 1), jnp.broadcast_to(jnp.exp(log_step[...]), (groups, groups)), 0.0)
    return jnp.sum(base, axis=1, keepdims=True)


def prepare_inverse(decay, frequency, group, scratch):
    groups = decay.shape[0]
    d, f = decay[...], frequency[...]
    modulus = d * d + f * f
    each = jnp.where(iota((groups * group, groups), 0) // group == iota((groups * group, groups), 1), 1.0, 0.0)
    scratch[0], scratch[1] = exact(each, d / modulus), exact(each, -f / modulus)


def prepare_inputs(inverse, input_real, input_imag, in_r, in_i):
    x_r, x_i = input_real[...], input_imag[...]
    in_r[...] = (x_r * inverse[0] - x_i * inverse[1]).astype(BF16)
    in_i[...] = (x_r * inverse[1] + x_i * inverse[0]).astype(BF16)


def prepare_skip(skip_gain, skip):
    group, groups = skip_gain.shape
    chans = groups * group
    each = jnp.where(iota((groups, chans), 0) == iota((groups, chans), 1) // group, 1.0, 0.0)
    keep = iota((group, chans), 0) == iota((group, chans), 1) % group
    skip[...] = jnp.sum(jnp.where(keep, exact(skip_gain[...], each), 0.0), axis=0, keepdims=True)


def own_states(row, sp, share, groups, states):
    flat = groups * states
    shape = (SUB, flat)
    mine = jnp.where(iota(shape, 1) % states == sp * share + iota(shape, 0), jnp.broadcast_to(row, shape), 0.0)
    each = jnp.where(iota((groups, flat), 0) == iota((groups, flat), 1) // states, 1.0, 0.0)
    return exact(mine, each, ((1,), (1,)))[0:share, :]


MESH = pl.DeviceIdType.MESH
HALO = 16
AHEAD = 5
SLOTS = 16


def pieces_of(shard):
    return 2 if shard >= 64 else 1


S, V, I, O, SO, CO = range(6)


def layer_kernel(sizes, *refs):
    n_sp, n_fs, n_tp, group, states = sizes
    inputs, (out, final), scratch = refs[:19], refs[19:21], refs[21:]
    hbm_weights, hbm_rest = inputs[:6], inputs[6:]
    local, scratch = scratch[:13], scratch[13:]
    (
        full, normed, state_p, hr, hi, ar, ai, pre, level, near, inbox, passed, reach_map, fin_src, fin_dst, ext, halo,
        conv_mix, state_mix, partial, got, rate, coef, opening, in_r, in_i, rd_r, rd_i, skip, inverse,
        load, load_w, ring_send, ring_recv, sib_send, sib_recv, near_send, near_recv, chain_send, chain_recv, map_send, map_recv, fin_send, fin_recv,
        x_send, x_recv, halo_send, halo_recv, mix_send, mix_recv,
    ) = scratch
    tokens, gain, log_step, decay, frequency, step_rate, input_real, input_imag, read_real, read_imag, skip_gain, taps, initial = local
    shard = hbm_weights[0].shape[0]
    rows = tokens.shape[0]
    channels = hbm_weights[0].shape[1]
    sp, fs, tp = lax.axis_index("sp"), lax.axis_index("fs"), lax.axis_index("tp")
    pairs = n_sp * n_fs // 2
    half = pairs // 2
    parts = pieces_of(shard)
    piece = shard // parts
    inner = math.gcd(n_sp, 4)
    outer = n_sp // inner
    here, layer = sp % inner, sp // inner
    mine = sp * n_fs + fs
    parity, chip = mine % 2, mine // 2
    place = jnp.where(chip % 2 == 0, chip // 2, pairs - 1 - chip // 2)

    def own(w):
        return full.at[w, pl.ds(pl.multiple_of(mine * shard, shard), shard), :]

    loads = [pltpu.make_async_copy(src, own(w), load_w.at[w]) for w, src in enumerate(hbm_weights)]
    rest = [pltpu.make_async_copy(src, dst, load.at[k]) for k, (src, dst) in enumerate(zip(hbm_rest, local))]
    for copy in loads[:2] + rest[:1] + loads[2:] + rest[1:]:
        copy.start()

    def pair_at(offset):
        q = (place + offset + pairs) % pairs
        return jnp.where(q < half, q * 2, (pairs - 1 - q) * 2 + 1)

    def device(linear):
        return (linear // n_fs, linear % n_fs, tp)

    neighbours = (device(pair_at(1) * 2 + parity), device(pair_at(-1) * 2 + parity))
    sibling = device(chip * 2 + 1 - parity)
    stages = inner.bit_length() - 1
    late = [(here >> k) % 2 == 1 for k in range(stages)]
    near_peers = [(sp + jnp.where(late[k], -1, 1) * (1 << k), fs, tp) for k in range(stages)]
    above = ((sp + inner) % n_sp, fs, tp)
    below = [(sp - s * inner + n_sp) % n_sp for s in range(1, outer)]
    after = ((sp + 1) % n_sp, fs, tp)
    tp_peers = [(sp, fs, (tp + s) % n_tp) for s in range(1, n_tp)]

    barrier = pltpu.get_barrier_semaphore()
    across = [(sibling[0], sibling[1], (tp + s) % n_tp) for s in range(n_tp)]
    greet = list(neighbours) + tp_peers + across
    for other in greet:
        pl.semaphore_signal(barrier, inc=1, device_id=other, device_id_type=MESH)
    pl.semaphore_wait(barrier, len(greet))

    def remote(src, dst, s_sem, r_sem, to):
        return pltpu.make_async_remote_copy(src_ref=src, dst_ref=dst, send_sem=s_sem, recv_sem=r_sem, device_id=to, device_id_type=MESH)

    def send(src, dst, s_sem, r_sem, to):
        remote(src, dst, s_sem, r_sem, to).start()

    def landed(ref, r_sem):
        remote(ref, ref, r_sem, r_sem, sibling).wait_recv()

    def gone(ref, s_sem):
        remote(ref, ref, s_sem, s_sem, sibling).wait_send()

    def slot(w, pair, par, h):
        return full.at[w, pl.ds(pl.multiple_of((pair * 2 + par) * shard + h * piece, piece), piece), :]

    def rounds(w, way):
        return half if way == w % 2 else pairs - 1 - half

    def source(way, r):
        return pair_at(-1 - r if way == 0 else 1 + r)

    def ways(w, r):
        return [way for way in range(2) if r < rounds(w, way)]

    def rows_of(w, count):
        return full.at[w, pl.ds(0, count), :]

    last_round = half - 1
    filler = [(V, r, h) for r in range(half) for h in range(parts)]
    pieces = []
    for r in range(half):
        pieces += [(S, r, h) for h in range(parts)] + filler[:1]
        del filler[:1]
    outputs = [(w, r) for r in range(half) for w in (SO, CO)]

    def both(*units):
        return [(w, r, h) for w, r in units for h in range(parts)]

    for r in range(half):
        if r < last_round:
            pieces += both((I, r), (O, r)) + filler[:parts]
            del filler[:parts]
        else:
            pieces += filler + both(outputs[0], (I, r), (O, r), *outputs[1:])
    where = {item: k for k, item in enumerate(pieces)}
    sent_to, seen = [0], [0]

    def send_piece(w, r, h):
        if r == 0 and h == 0:
            loads[w].wait()
        for way in ways(w, r):
            at = chip if r == 0 else source(way, r - 1)
            ref = slot(w, at, parity, h)
            send(ref, ref, ring_send.at[w], ring_recv.at[where[w, r, h] % SLOTS], neighbours[way])
        if r == 0 and h == parts - 1 and w < SO:
            send(own(w), own(w), sib_send.at[w], sib_recv.at[w], sibling)

    def feed():
        while sent_to[0] < len(pieces) and sent_to[0] <= seen[0] + AHEAD:
            w, r, h = pieces[sent_to[0]]
            if r > 0 and where[w, r - 1, h] >= seen[0]:
                break
            send_piece(w, r, h)
            sent_to[0] += 1

    def pump(count=1):
        for _ in range(count):
            if seen[0] == len(pieces):
                return
            w, r, h = pieces[seen[0]]
            landed(rows_of(w, len(ways(w, r)) * piece), ring_recv.at[seen[0] % SLOTS])
            seen[0] += 1
            feed()
            for way in ways(w, r) if w < SO else ():
                ref = slot(w, source(way, r), parity, h)
                send(ref, ref, sib_send.at[w], sib_recv.at[w], sibling)

    def until(w, r):
        pump(max(0, where[w, r, parts - 1] + 1 - seen[0]))

    def finish(w):
        until(w, last_round)
        landed(rows_of(w, pairs * shard), sib_recv.at[w])

    feed()
    rest[0].wait()
    rest[1].wait()

    def normalize(x):
        x = x.astype(F32)
        scale = lax.rsqrt(jnp.mean(x * x, axis=-1, keepdims=True) + 1e-06)
        return (x * scale * gain[...]).astype(BF16)

    def norm(j, carry):
        at = pl.multiple_of(j * 32, 32)
        normed[pl.ds(HALO + at, 32), :] = normalize(tokens[pl.ds(at, 32), :])
        return carry

    lax.fori_loop(0, rows // 32, norm, 0)
    for copy in rest[2:]:
        copy.wait()
    pump()
    perm = permutation(rows)
    prepare_rates(step_rate, rate)
    pump()
    prepare_inverse(decay, frequency, group, inverse)
    pump()
    prepare_inputs(inverse, input_real, input_imag, in_r, in_i)
    pump()
    base = prepare_base(log_step, decay.shape[0])
    coef[0:1, :], coef[1:2, :] = flatten([base * decay[...], base * frequency[...] * 0.15915494309189535], states)
    pump()
    opening[0:1, :], opening[1:2, :] = flatten([initial[0 : decay.shape[0], :], initial[decay.shape[0] :, :]], states)
    pump()
    rd_r[...] = read_real[...].astype(BF16)
    rd_i[...] = read_imag[...].astype(BF16)
    prepare_skip(skip_gain, skip)
    finish(S)

    def project(w):
        return dot(normed[HALO:, :], full[w]).astype(BF16)

    def project_more(w):
        return dot(normed[...], full[w]).astype(BF16)

    send(tokens.at[pl.ds(rows - SUB, SUB), :], halo, halo_send, halo_recv, after)
    state_p[...] = dot(perm, project(S)).astype(BF16)
    pump(2)
    width = min(128, channels)
    span = width // group * states
    blocks = channels // width
    for block in range(blocks):
        couple(block, state_p[:, block * width : (block + 1) * width], in_r, in_i, hr, hi, group, states)
        scan_block(block * span, span, rate, coef, hr, hi, ar, ai)
        pump(1 + block % 2)
    chain_subs(hr, hi, ar, ai, pre, level.at[0])

    def meet(k):
        landed(near.at[k], near_recv.at[k])
        mine_k, theirs = level[k], near[k]
        level[k + 1] = join(jnp.where(late[k], theirs, mine_k), jnp.where(late[k], mine_k, theirs))

    middle = outer // 2

    def pass_state(start, t):
        fin_src[0:1, :], fin_src[1:2, :] = enter(level[stages], start[0:1, :], start[1:2, :])
        for d in range(1, outer if t == middle - 1 else 2):
            if t + d < outer:
                up = ((sp + d * inner) % n_sp, fs, tp)
                remote(fin_src, inbox, chain_send.at[d - 1], chain_recv, up).start()

    def carry_low(t):
        @pl.when(layer == t)
        def _():
            if t > 0:
                landed(inbox, chain_recv)
            pass_state(inbox if t > 0 else opening, t)

    def carry_high(t):
        @pl.when(layer == t)
        def _():
            if t == middle:
                reach_map[...] = level[stages]
            else:
                landed(passed, map_recv)
                reach_map[...] = join(passed[...], level[stages])
            if t < outer - 1:
                remote(reach_map, passed, map_send, map_recv, above).start()

    for k in range(stages):
        send(level.at[k], near.at[k], near_send.at[k], near_recv.at[k], near_peers[k])
        pump(2 + k)
        meet(k)
    carry_low(0)
    carry_high(middle)
    pump(2)
    landed(halo, halo_recv)
    normed[:HALO, :] = jnp.concatenate([jnp.zeros((HALO - SUB, halo.shape[1]), BF16), normalize(halo[...])], axis=0)
    finish(V)
    value = project_more(V)
    pump(2)
    for t in range(1, middle):
        carry_low(t)
        carry_high(middle + t)
        pump(3)
    last = layer == outer - 1

    @pl.when(layer >= middle)
    def _():
        landed(inbox, chain_recv)

    @pl.when(last)
    def _():
        fin_src[0:1, :], fin_src[1:2, :] = enter(reach_map, inbox[0:1, :], inbox[1:2, :])
        for s, other in enumerate(below):
            remote(fin_src, fin_dst, fin_send.at[s], fin_recv, (other, fs, tp)).start()

    e_r = jnp.where(layer == 0, opening[0:1, :], inbox[0:1, :])
    e_i = jnp.where(layer == 0, opening[1:2, :], inbox[1:2, :])
    t_r, t_i = enter(passed, e_r, e_i)
    e_r, e_i = jnp.where(layer > middle, t_r, e_r), jnp.where(layer > middle, t_i, e_i)
    for k in reversed(range(stages)):
        t_r, t_i = enter(near[k], e_r, e_i)
        e_r, e_i = jnp.where(late[k], t_r, e_r), jnp.where(late[k], t_i, e_i)
    for block in range(blocks):
        readout(block, width, state_p, (e_r, e_i), hr, hi, ar, ai, pre, rd_r, rd_i, skip, perm, state_mix.at[parity], group, states)
        if block % 2 == 1:
            pump()

    send(state_mix.at[parity], state_mix.at[parity], mix_send.at[0], mix_recv.at[0], sibling)
    until(I, last_round)
    pump(2)
    finish(I)
    product = project_more(I).astype(F32) * value.astype(F32)
    product = jnp.where(jnp.logical_and(sp == 0, iota(product.shape, 0) < HALO), 0.0, product)
    ext[...] = product.astype(BF16).astype(F32)
    pump()
    finish(O)
    outward = project(O)
    reach = taps.shape[0] - 1
    filtered = taps[0:1, :] * ext[HALO - reach : HALO - reach + rows, :]
    for tap in range(1, reach + 1):
        at = HALO - reach + tap
        filtered = filtered + taps[tap : tap + 1, :] * ext[at : at + rows, :]
    conv_mix[parity] = (outward.astype(F32) * filtered).astype(BF16)
    own_rows = rows // n_tp
    chunks = []

    def columns(pair, par):
        return pl.ds(pl.multiple_of((pair * 2 + par) * shard, shard), shard)

    def out_rows(pairs_now, mixes):
        weights = [jnp.concatenate([full[w, columns(pair, parity), :] for pair in pairs_now], axis=0) for w in (SO, CO)]
        return sum(dot(mix, w, ((1,), (1,))) for mix, w in zip(mixes, weights)).astype(BF16)

    def compute(some):
        total = out_rows(some, [mix[...].reshape(2 * rows, mix.shape[2]) for mix in (state_mix, conv_mix)])
        for k, pair in enumerate(some):
            partial[pl.ds(pair, 1)] = total[:, k * shard : (k + 1) * shard][None]

    def compute_core(some, core):
        total = out_rows(some, [state_mix[core], conv_mix[core]])
        for k, pair in enumerate(some):
            partial[pair, pl.ds(pl.multiple_of(core * rows, rows), rows), :] = total[:, k * shard : (k + 1) * shard]

    def compute_share(pair, t):
        at = pl.ds(pl.multiple_of(t * own_rows, own_rows), own_rows)
        total = out_rows([pair], [mix[:, at, :].reshape(2 * own_rows, mix.shape[2]) for mix in (state_mix, conv_mix)])
        for core in range(2):
            spot = pl.ds(pl.multiple_of(core * rows + t * own_rows, own_rows), own_rows)
            partial[pair, spot, :] = total[core * own_rows : (core + 1) * own_rows, :]

    def exchange(pair, cores=(0, 1), shares=None):
        if all(pair is not done for done in chunks):
            chunks.append(pair)
        order = [pair is done for done in chunks].index(True)
        for s in range(n_tp) if shares is None else shares:
            for core in cores:
                if s + core > 0:
                    other = (tp + s) % n_tp
                    at = (parity if core == 0 else 1 - parity) * rows + other * own_rows
                    theirs = partial.at[pair, pl.ds(pl.multiple_of(at, own_rows), own_rows), :]
                    to = across[s] if core else (sp, fs, other)
                    send(theirs, got.at[pair, core * (n_tp - 1) + s - 1 + core], x_send, x_recv.at[order], to)

    first = [source(way, 0) for way in ways(SO, 0)]
    compute_core([chip], parity)
    send(conv_mix.at[parity], conv_mix.at[parity], mix_send.at[1], mix_recv.at[1], sibling)
    exchange(chip, cores=(0,))
    until(SO, 0)
    until(CO, 0)
    compute_core(first, parity)
    for pair in first:
        exchange(pair, cores=(0,))
    pump()
    for k, mix in enumerate((state_mix, conv_mix)):
        landed(mix.at[1 - parity], mix_recv.at[k])
    compute_core([chip], 1 - parity)
    exchange(chip, cores=(1,))
    pump()
    compute_core(first, 1 - parity)
    for pair in first:
        exchange(pair, cores=(1,))
    pump()
    for r in range(1, last_round):
        until(SO, r)
        until(CO, r)
        fresh = [source(way, r) for way in ways(SO, r)]
        compute(fresh)
        for pair in fresh:
            exchange(pair)
        pump()
    until(SO, last_round)
    until(CO, last_round)
    final_pair = source(0, last_round)
    for s in (*range(1, n_tp), 0):
        compute_share(final_pair, (tp + s) % n_tp)
        exchange(final_pair, shares=(s,))

    @pl.when(jnp.logical_not(last))
    def _():
        landed(fin_dst, fin_recv)

    share_states = states // n_sp
    groups = decay.shape[0]
    for k in range(2):
        row = jnp.where(last, fin_src[k : k + 1, :], fin_dst[k : k + 1, :])
        final[k] = own_states(row, sp, share_states, groups, states)
    kept = pl.ds(pl.multiple_of(parity * rows + tp * own_rows, own_rows), own_rows)

    def settle(k):
        ours, theirs = partial[k, kept, :].astype(F32), got[k, n_tp - 1].astype(F32)
        for s in range(1, n_tp):
            ours = ours + got[k, s - 1].astype(F32)
            theirs = theirs + got[k, n_tp - 1 + s].astype(F32)
        return ours.astype(BF16), theirs.astype(BF16)

    for c, pair in enumerate(chunks):
        landed(got.at[pair], x_recv.at[c])
        if shard % 128 == 0:
            out[:, columns(pair, parity)], out[:, columns(pair, 1 - parity)] = settle(pair)
    if shard % 128:
        for k in range(pairs):
            ours, theirs = settle(k)
            out[:, k * 2 * shard : (k * 2 + 1) * shard] = jnp.where(parity == 0, ours, theirs)
            out[:, (k * 2 + 1) * shard : (k + 1) * 2 * shard] = jnp.where(parity == 0, theirs, ours)
    for w in range(6):
        gone(rows_of(w, (pairs - 1) * shard), ring_send.at[w])
        if w < SO:
            gone(rows_of(w, pairs * shard), sib_send.at[w])
    for k in range(stages):
        gone(near.at[k], near_send.at[k])
    gone(halo, halo_send)
    gone(got, x_send)
    for k, mix in enumerate((state_mix, conv_mix)):
        gone(mix.at[parity], mix_send.at[k])

    for d in range(1, outer):
        senders = layer < middle if d == 1 else layer == middle - 1
        if d < outer - middle + 1:

            @pl.when(senders)
            def _():
                gone(fin_src, chain_send.at[d - 1])

    if outer - 1 > middle:

        @pl.when(jnp.logical_and(layer >= middle, layer < outer - 1))
        def _():
            gone(reach_map, map_send)

    for s in range(outer - 1):

        @pl.when(last)
        def _():
            gone(fin_src, fin_send.at[s])


def body(tokens, norm_gain, w_state_in, w_value, w_outer, w_inner, w_state_out, w_conv_out, log_step, decay_real, frequency, step_rate, input_real, input_imag, read_real, read_imag, skip_gain, conv_taps, initial_state):
    rows, features = tokens.shape[1:]
    groups, states = decay_real.shape
    group = skip_gain.shape[1]
    flat = groups * states
    channels = groups * group
    conv = conv_taps.shape[1]
    n_sp, n_fs, n_tp = (lax.axis_size(a) for a in ("sp", "fs", "tp"))
    shard = w_state_in.shape[0]
    pairs = n_sp * n_fs // 2
    half = pairs // 2
    inner = math.gcd(n_sp, 4)
    outer = n_sp // inner
    share = states // n_sp
    parts = pieces_of(shard)
    weights = (w_state_in, w_value, w_inner, w_outer, w_state_out, w_conv_out)
    rest = (
        tokens[0], norm_gain[None], log_step[None], decay_real, frequency, step_rate,
        jnp.swapaxes(input_real, 1, 2).reshape(channels, states), jnp.swapaxes(input_imag, 1, 2).reshape(channels, states),
        read_real.reshape(channels, states), read_imag.reshape(channels, states), skip_gain.T, conv_taps,
        initial_state.reshape(2 * groups, states),
    )
    vmem = pltpu.VMEM
    dma = pltpu.SemaphoreType.DMA
    out, final = pl.pallas_call(
        lambda *refs: layer_kernel((n_sp, n_fs, n_tp, group, states), *refs),
        out_shape=(jax.ShapeDtypeStruct((rows // n_tp, features), BF16), jax.ShapeDtypeStruct((2, share, groups), F32)),
        in_specs=[pl.BlockSpec(memory_space=pltpu.HBM)] * 19,
        out_specs=[pl.BlockSpec(memory_space=vmem)] * 2,
        scratch_shapes=[
            *[vmem(a.shape, a.dtype) for a in rest],
            vmem((6, n_sp * n_fs * shard, channels), BF16),
            vmem((HALO + rows, features), BF16),
            vmem((rows, channels), BF16),
            *[vmem((rows, flat), F32)] * 4,
            vmem((4, SUB, flat), F32),
            vmem((inner.bit_length(), 4, flat), F32),
            vmem((inner.bit_length() - 1, 4, flat), F32),
            vmem((2, flat), F32),
            vmem((4, flat), F32),
            vmem((4, flat), F32),
            vmem((2, flat), F32),
            vmem((2, flat), F32),
            vmem((rows + HALO, conv), F32),
            vmem((SUB, features), BF16),
            vmem((2, rows, conv), BF16),
            vmem((2, rows, channels), BF16),
            vmem((pairs, 2 * rows, shard), BF16),
            vmem((pairs, 2 * n_tp - 1, rows // n_tp, shard), BF16),
            vmem((rows, 128), F32),
            vmem((2, flat), F32),
            vmem((2, flat), F32),
            *[vmem((channels, states), BF16)] * 4,
            vmem((1, channels), F32),
            vmem((2, channels, states), F32),
            dma((13,)),
            dma((6,)),
            dma((6,)),
            dma((SLOTS,)),
            dma((SO,)),
            dma((SO,)),
            dma((inner.bit_length() - 1,)),
            dma((inner.bit_length() - 1,)),
            dma((outer - 1,)),
            dma,
            dma,
            dma,
            dma((outer - 1,)),
            dma,
            dma,
            dma((pairs,)),
            dma,
            dma,
            dma((2,)),
            dma((2,)),
        ],
        compiler_params=pltpu.CompilerParams(collective_id=0, has_side_effects=True, vmem_limit_bytes=36 * 1024 * 1024),
        name="layer",
    )(*(pltpu.with_memory_space_constraint(a, pltpu.HBM) for a in weights + rest))
    return out[None], jnp.swapaxes(final, 1, 2)[None]


def solution(mesh):
    return jax.shard_map(
        body,
        mesh=mesh,
        in_specs=(
            P("fs", "sp", None),
            P(),
            P(("sp", "fs"), "tp"),
            P(("sp", "fs"), "tp"),
            P(("sp", "fs"), "tp"),
            P(("sp", "fs"), "tp"),
            P(("sp", "fs"), "tp"),
            P(("sp", "fs"), "tp"),
            P("tp"),
            P("tp", None),
            P("tp", None),
            P("fs", "sp"),
            P("tp", None, None),
            P("tp", None, None),
            P("tp", None, None),
            P("tp", None, None),
            P("tp", None),
            P(None, "tp"),
            P("fs", None, "tp", None),
        ),
        out_specs=(P("fs", ("sp", "tp"), None), P("fs", None, "tp", "sp")),
        check_vma=False,
    )
```

profile of v0, /device:TPU:0, one launch (start us, length us, event | category | flops | bytes accessed | tf_op | source)
XLA Modules:
  0.0 72.6 jit_solution(13852141653101028304)
XLA Ops:
  0.6 70.5 %layer.1 = (bf16[128,2048]{1,0:T(8,128)(2,1)S(1)}, f32[2,4,32]{2,1,0:T(4,128)S(1)}) custom-call(bf16[128,512]{1,0:T(8,128)(2,1)} %refs_0_.1, bf16[128,512]{1,0:T(8,128)(2,1)} %refs_1_.1, bf16[128,512]{1,0:T(8,128)(2,1)} %refs_2_.1, bf16[128,512]{1,0:T(8,128)(2,1)} %refs_3_.1, bf16[128,512]{1,0:T(8,128)(2,1)} %refs_4_.1, bf16[128,512]{1,0:T(8,128)(2,1)} %refs_5_.1, ...), custom_call_target="tpu_custom_call" | custom-call | tf_op jit(solution)/shard_map/layer/pallas_call | solution.py:651
  71.2 0.8 %copy.23 = bf16[1,128,2048]{2,1,0:T(8,128)(2,1)} copy(bf16[1,128,2048]{2,1,0:T(8,128)(2,1)S(1)} %bitcast.17) | data formatting | bytes 1048576
  72.0 0.6 copy.24
where the time goes:
time: 72.7 us; the launch traced here: 72.6 us
  Pallas kernels  70.5 us (97%)
  local copies, waits for them, and re-layouts  1.39 us (2%)
    pallas_call x1, Pallas kernels, body(): pl.pallas_call(lambda *refs: layer_kernel((n_sp, n_fs, n_tp, group, state...  70.5 us

commit v1 on v0

--- a/solution.py
+++ b/solution.py
@@ -319,9 +319,9 @@
         for way in ways(w, r):
             at = chip if r == 0 else source(way, r - 1)
             ref = slot(w, at, parity, h)
-            send(ref, ref, ring_send.at[w], ring_recv.at[where[w, r, h] % SLOTS], neighbours[way])
+            send(ref, ref, ring_send, ring_recv.at[where[w, r, h] % SLOTS], neighbours[way])
         if r == 0 and h == parts - 1 and w < SO:
-            send(own(w), own(w), sib_send.at[w], sib_recv.at[w], sibling)
+            send(own(w), own(w), sib_send, sib_recv.at[w], sibling)
 
     def feed():
         while sent_to[0] < len(pieces) and sent_to[0] <= seen[0] + AHEAD:
@@ -341,7 +341,7 @@
             feed()
             for way in ways(w, r) if w < SO else ():
                 ref = slot(w, source(way, r), parity, h)
-                send(ref, ref, sib_send.at[w], sib_recv.at[w], sibling)
+                send(ref, ref, sib_send, sib_recv.at[w], sibling)
 
     def until(w, r):
         pump(max(0, where[w, r, parts - 1] + 1 - seen[0]))
@@ -501,8 +501,12 @@
         weights = [jnp.concatenate([full[w, columns(pair, parity), :] for pair in pairs_now], axis=0) for w in (SO, CO)]
         return sum(dot(mix, w, ((1,), (1,))) for mix, w in zip(mixes, weights)).astype(BF16)
 
-    def compute(some):
-        total = out_rows(some, [mix[...].reshape(2 * rows, mix.shape[2]) for mix in (state_mix, conv_mix)])
+    def out_part(some, mix, w):
+        weight = jnp.concatenate([full[w, columns(pair, parity), :] for pair in some], axis=0)
+        return dot(mix[...].reshape(2 * rows, mix.shape[2]), weight, ((1,), (1,)))
+
+    def compute(some, state_part):
+        total = (state_part + out_part(some, conv_mix, CO)).astype(BF16)
         for k, pair in enumerate(some):
             partial[pl.ds(pair, 1)] = total[:, k * shard : (k + 1) * shard][None]
 
@@ -511,9 +515,12 @@
         for k, pair in enumerate(some):
             partial[pair, pl.ds(pl.multiple_of(core * rows, rows), rows), :] = total[:, k * shard : (k + 1) * shard]
 
-    def compute_share(pair, t):
+    def share_rows(mix, t):
         at = pl.ds(pl.multiple_of(t * own_rows, own_rows), own_rows)
-        total = out_rows([pair], [mix[:, at, :].reshape(2 * own_rows, mix.shape[2]) for mix in (state_mix, conv_mix)])
+        return mix[:, at, :].reshape(2 * own_rows, mix.shape[2])
+
+    def finish_share(pair, t, state_part):
+        total = (state_part + dot(share_rows(conv_mix, t), full[CO, columns(pair, parity), :], ((1,), (1,)))).astype(BF16)
         for core in range(2):
             spot = pl.ds(pl.multiple_of(core * rows + t * own_rows, own_rows), own_rows)
             partial[pair, spot, :] = total[core * own_rows : (core + 1) * own_rows, :]
@@ -552,17 +559,20 @@
     pump()
     for r in range(1, last_round):
         until(SO, r)
+        fresh = [source(way, r) for way in ways(SO, r)]
+        state_part = out_part(fresh, state_mix, SO)
         until(CO, r)
-        fresh = [source(way, r) for way in ways(SO, r)]
-        compute(fresh)
+        compute(fresh, state_part)
         for pair in fresh:
             exchange(pair)
         pump()
     until(SO, last_round)
+    final_pair = source(0, last_round)
+    order = [(s, (tp + s) % n_tp) for s in (*range(1, n_tp), 0)]
+    state_parts = [dot(share_rows(state_mix, t), full[SO, columns(final_pair, parity), :], ((1,), (1,))) for _, t in order]
     until(CO, last_round)
-    final_pair = source(0, last_round)
-    for s in (*range(1, n_tp), 0):
-        compute_share(final_pair, (tp + s) % n_tp)
+    for (s, t), state_part in zip(order, state_parts):
+        finish_share(final_pair, t, state_part)
         exchange(final_pair, shares=(s,))
 
     @pl.when(jnp.logical_not(last))
@@ -592,10 +602,8 @@
             ours, theirs = settle(k)
             out[:, k * 2 * shard : (k * 2 + 1) * shard] = jnp.where(parity == 0, ours, theirs)
             out[:, (k * 2 + 1) * shard : (k + 1) * 2 * shard] = jnp.where(parity == 0, theirs, ours)
-    for w in range(6):
-        gone(rows_of(w, (pairs - 1) * shard), ring_send.at[w])
-        if w < SO:
-            gone(rows_of(w, pairs * shard), sib_send.at[w])
+    gone(full.at[:, pl.ds(0, (pairs - 1) * shard), :], ring_send)
+    gone(full.at[pl.ds(0, SO), pl.ds(0, pairs * shard), :], sib_send)
     for k in range(stages):
         gone(near.at[k], near_send.at[k])
     gone(halo, halo_send)
@@ -681,9 +689,9 @@
             vmem((2, channels, states), F32),
             dma((13,)),
             dma((6,)),
-            dma((6,)),
+            dma,
             dma((SLOTS,)),
-            dma((SO,)),
+            dma,
             dma((SO,)),
             dma((inner.bit_length() - 1,)),
             dma((inner.bit_length() - 1,)),

time: 72.7 us -> 72.6 us (level)
  no operation moved by 1% of the time
where the time goes in v1:
time: 72.6 us; the launch traced here: 72.5 us
  Pallas kernels  70.5 us (97%)
  local copies, waits for them, and re-layouts  1.39 us (2%)
    pallas_call x1, Pallas kernels, body(): pl.pallas_call(lambda *refs: layer_kernel((n_sp, n_fs, n_tp, group, state...  70.5 us

profile of v1, /device:TPU:0, one launch (start us, length us, event | category | flops | bytes accessed | tf_op | source)
XLA Modules:
  0.0 72.5 jit_solution(528246623397319644)
XLA Ops:
  0.6 70.5 %layer.1 = (bf16[128,2048]{1,0:T(8,128)(2,1)S(1)}, f32[2,4,32]{2,1,0:T(4,128)S(1)}) custom-call(bf16[128,512]{1,0:T(8,128)(2,1)} %refs_0_.1, bf16[128,512]{1,0:T(8,128)(2,1)} %refs_1_.1, bf16[128,512]{1,0:T(8,128)(2,1)} %refs_2_.1, bf16[128,512]{1,0:T(8,128)(2,1)} %refs_3_.1, bf16[128,512]{1,0:T(8,128)(2,1)} %refs_4_.1, bf16[128,512]{1,0:T(8,128)(2,1)} %refs_5_.1, ...), custom_call_target="tpu_custom_call" | custom-call | tf_op jit(solution)/shard_map/layer/pallas_call | solution.py:659
  71.1 0.8 %copy.23 = bf16[1,128,2048]{2,1,0:T(8,128)(2,1)} copy(bf16[1,128,2048]{2,1,0:T(8,128)(2,1)S(1)} %bitcast.17) | data formatting | bytes 1048576
  71.9 0.6 copy.24
